TPU v7x, 32 devices: a whole 2x2x4 slice. The times are simulated.
32 devices in a mesh: ep: 8 (over z, x), tp: 4 (over y, core).
Axes of the slice: x: 2, y: 2, z: 4, core: 2. Of those that a mesh axis runs over, the one named last changes fastest.
Arguments:
- conv_input: bfloat16 [8192, 2048], P('ep', 'tp'), may hold values from -6 to 6
- conv_kernel: bfloat16 [31, 2048], P(None, 'tp'), may hold values from -2 to 2
- norm_gain: float32 [2048], P('tp'), may hold values from 0.1 to 1.9
- norm_shift: float32 [2048], P('tp'), may hold values from -3 to 3
- conv_proj: bfloat16 [2048, 2048], P('tp'), may hold values from -0.125 to 0.125
- moe_input: bfloat16 [2048, 2048], P(('ep', 'tp')), may hold values from -6 to 6
- moe_gain: float32 [2048], replicated, may hold values from 0.1 to 1.9
- routes: int32 [2048, 2], P('ep'), may hold values from 0 to 7, all different within a row; in each aligned block of 256 rows (0 to 255, 256 to 511, ...) at most 128 rows name the same one
- route_weights: float32 [2048, 2], P('ep'), may hold values from 0.2 to 1
- gate_proj: bfloat16 [8, 2048, 2048], P('ep', None, 'tp'), may hold values from -0.125 to 0.125
- up_proj: bfloat16 [8, 2048, 2048], P('ep', None, 'tp'), may hold values from -0.125 to 0.125
- down_proj: bfloat16 [8, 2048, 2048], P('ep', 'tp'), may hold values from -0.125 to 0.125
Outputs:
- conv_out: bfloat16 [8192, 2048], P(('ep', 'tp'))
- moe_out: bfloat16 [2048, 2048], P(('ep', 'tp'))
Inputs may be any that keep to these rules, and one draw needn't show every extreme that they name: `routes`: each row names 2 different experts. In each aligned block of 256 rows no expert is named by more than 128 rows, and in some blocks an expert is named by exactly 128 rows.
All inputs are finite; a program needn't handle non-finite values.
Results may differ from a plain program's by a relative error of at most 0.012.
Values may be sent and summed in bfloat16 or wider, within the bound.
A program may use at most 128 MiB of HBM per device.

v0:
```python
import jax
import jax.numpy as jnp
from jax import lax
from jax.sharding import PartitionSpec as P


def shifted(value, axis, steps):
    count = lax.axis_size(axis)
    leading, last = (max(0, -steps), min(count, count - steps))
    return lax.ppermute(value, axis, [(source, source + steps) for source in range(leading, last)])


def local(
    conv_input,
    conv_kernel,
    norm_gain,
    norm_shift,
    conv_proj,
    moe_input,
    moe_gain,
    routes,
    route_weights,
    gate_proj,
    up_proj,
    down_proj,
):
    tp_count = lax.axis_size("tp")
    ep_count = lax.axis_size("ep")
    local_rows, local_width = conv_input.shape
    reach = conv_kernel.shape[0] - 1
    history = shifted(conv_input[local_rows - reach :], "ep", 1)
    padded = jnp.concatenate([history, conv_input], axis=0)
    taps = conv_kernel.astype(jnp.float32)
    mixed = jnp.zeros((local_rows, local_width), jnp.float32)
    for offset in range(reach + 1):
        mixed = mixed + padded[offset : offset + local_rows].astype(jnp.float32) * taps[offset]
    full_width = local_width * tp_count
    sums, squares = lax.psum((jnp.sum(mixed, axis=1), jnp.sum(mixed * mixed, axis=1)), "tp")
    center = sums / full_width
    spread = jnp.maximum(squares / full_width - center * center, 0.0)
    scaled = (mixed - center[:, None]) * lax.rsqrt(spread[:, None] + 1e-05) * norm_gain + norm_shift
    activated = jax.nn.silu(scaled).astype(jnp.bfloat16)
    conv_out = lax.psum_scatter(
        jnp.dot(activated, conv_proj, preferred_element_type=jnp.float32).astype(jnp.bfloat16),
        "tp",
        scatter_dimension=0,
        tiled=True,
    )
    moe_float = moe_input.astype(jnp.float32)
    normed = (
        moe_float
        * lax.rsqrt(jnp.mean(moe_float * moe_float, axis=1, keepdims=True) + 1e-06)
        * moe_gain
    ).astype(jnp.bfloat16)
    group = lax.all_gather(normed, "tp", axis=0, tiled=True)
    group_rows, top_count = routes.shape
    model_width = group.shape[1]
    capacity = 2 * top_count * group_rows // ep_count
    expert_ids = routes.reshape(-1)
    onehot = (expert_ids[:, None] == jnp.arange(ep_count, dtype=jnp.int32)[None, :]).astype(
        jnp.int32
    )
    ranks = jnp.sum((jnp.cumsum(onehot, axis=0) - onehot) * onehot, axis=1)
    targets = ranks * ep_count + expert_ids
    owners = jnp.arange(group_rows * top_count, dtype=jnp.int32) // top_count
    table = jnp.full((capacity * ep_count,), group_rows, jnp.int32).at[targets].set(owners)
    extended = jnp.concatenate([group, jnp.zeros((1, model_width), jnp.bfloat16)], axis=0)
    outgoing = extended[table].reshape(capacity, ep_count, model_width)
    share = capacity // tp_count
    own_slots = lax.dynamic_slice_in_dim(outgoing, lax.axis_index("tp") * share, share, 0)
    landed = lax.all_to_all(own_slots, "ep", split_axis=1, concat_axis=1, tiled=True)
    arrived = lax.all_gather(landed, "tp", axis=0, tiled=True)
    incoming = arrived.reshape(capacity * ep_count, model_width)
    gated = jax.nn.silu(jnp.dot(incoming, gate_proj[0], preferred_element_type=jnp.float32))
    hidden = (gated * jnp.dot(incoming, up_proj[0], preferred_element_type=jnp.float32)).astype(
        jnp.bfloat16
    )
    weights_flat = route_weights.reshape(-1)
    pieces = jnp.dot(hidden, down_proj[0], preferred_element_type=jnp.float32).astype(jnp.bfloat16)
    returned = lax.all_to_all(
        pieces.reshape(capacity, ep_count, model_width),
        "ep",
        split_axis=1,
        concat_axis=1,
        tiled=True,
    )
    picked = returned.reshape(-1, model_width)[targets].astype(jnp.float32)
    combined = jnp.sum(
        (picked * weights_flat[:, None]).reshape(group_rows, top_count, model_width), axis=1
    )
    moe_out = lax.psum_scatter(combined.astype(jnp.bfloat16), "tp", scatter_dimension=0, tiled=True)
    return (conv_out, moe_out)


def solution(mesh):
    placed = (
        P("ep", "tp"),
        P(None, "tp"),
        P("tp"),
        P("tp"),
        P("tp", None),
        P(("ep", "tp"), None),
        P(),
        P("ep", None),
        P("ep", None),
        P("ep", None, "tp"),
        P("ep", None, "tp"),
        P("ep", "tp", None),
    )
    return jax.shard_map(
        local,
        mesh=mesh,
        in_specs=placed,
        out_specs=(P(("ep", "tp"), None), P(("ep", "tp"), None)),
        check_vma=False,
    )
```

profile of v0, /device:TPU:0, one launch (start us, length us, event | category | flops | bytes accessed | tf_op | source)
XLA Modules:
  0.0 288.2 jit_solution(171710955497054303)
XLA Ops:
  7.2 0.0 copy-start
  7.2 0.0 all-gather.3.cloned.1.call-start
  7.2 1.2 fusion.50
  8.5 1.8 fusion.52
  10.3 0.0 all-gather.3.cloned.1.call-update
  10.3 0.0 all-gather.5.cloned.1.call-start
  10.4 0.8 copy.19
  11.2 0.1 eq.29
  11.3 0.1 eq.25
  11.5 0.1 reshape.90
  11.6 1.1 reduce-window.6
  12.8 0.2 slice_reduce_fusion
  13.0 0.1 fusion.54
  13.1 2.4 scatter_custom_fusion
  15.6 14.3 %all-gather.3.cloned.1.call-done = bf16[256,2048]{1,0:T(8,128)(2,1)} async-done(((bf16[64,2048]{1,0:T(8,128)(2,1)}), bf16[256,2048]{1,0:T(8,128)(2,1)}) %all-gather.3.cloned.1.call-update) | async-done | bytes 1048592 | tf_op jit(solution)/shard_map/all_gather | solution.py:55
  29.9 1.3 concatenate.7
  31.2 6.0 %gather_fusion = bf16[1024,2048]{1,0:T(8,128)(2,1)} fusion(bf16[257,2048]{1,0:T(8,128)(2,1)S(1)} %concatenate.7, s32[1024]{0:T(1024)S(1)} %fusion.56), kind=kCustom, calls=%fused_computation | custom fusion | bytes 8392704 | tf_op jit(solution)/shard_map/gather | solution.py:68
  37.2 1.3 constant_dynamic-slice_fusion
  38.5 0.6 copy.27
  39.1 31.4 %all_to_all.10 = bf16[32,8,2048]{2,0,1:T(8,128)(2,1)S(1)} all-to-all(bf16[32,8,2048]{2,0,1:T(8,128)(2,1)S(1)} %copy.27), channel_id=1, replica_groups=mesh['ep'=8,'tp'=4] {'ep'}, dimensions={1} | all-to-all | bytes 2097152 | tf_op jit(solution)/shard_map/all_to_all | solution.py:71
  70.5 1.6 copy.23
  72.1 0.0 all-gather.5.cloned.1.call-update
  72.1 0.0 reduce-scatter.3.cloned.1.call-start
  72.2 0.0 copy-done.1
  72.2 3.4 %collective-permute-start = (bf16[30,512]{1,0:T(8,128)(2,1)S(1)}, bf16[30,512]{1,0:T(8,128)(2,1)S(1)}, u32[]{:S(2)}, u32[]{:S(2)}) collective-permute-start(bf16[30,512]{1,0:T(8,128)(2,1)S(1)} %slice.192), channel_id=1, source_target_pairs={{0,4},{4,8},{8,12},{12,16},{16,20},{20,24},{24,28},{1,5},{5,9},{9,... | collective-permute-start | bytes 92168 | tf_op jit(solution)/shard_map/ppermute | solution.py:10
  75.6 0.0 copy-done.2
  75.6 1.5 collective-permute-done
  77.1 11.2 %fusion.64 = (f32[1024]{0:T(1024)S(1)}, f32[1024]{0:T(1024)S(1)}, f32[1024,512]{1,0:T(8,128)}) fusion(f32[512]{0:T(512)S(1)} %bitcast.105, bf16[1024,512]{1,0:T(8,128)(2,1)S(1)} %copy-done.1, f32[512]{0:T(512)S(1)} %bitcast.104, bf16[30,512]{1,0:T(8,128)(2,1)S(1)} %collective-permute-done, f32[512]{0:T(512)S(1)} %bitcast.103, f32[512]{0:T(512)S(1)} %bitcast.102, ...), kind=kLoop, calls=%fused_computation.119 | loop fusion | flops 96991232 | bytes 3248128 | tf_op jit(solution)/shard_map/reduce_sum | solution.py:38
  88.3 7.0 %all-reduce.1 = (f32[1024]{0:T(1024)S(1)}, f32[1024]{0:T(1024)S(1)}) all-reduce(f32[1024]{0:T(1024)S(1)} %get-tuple-element.3, f32[1024]{0:T(1024)S(1)} %get-tuple-element.2), channel_id=1, replica_groups=mesh['ep'=8,'tp'=4] {'tp'}, use_global_device_ids=true, to_apply=%region_3.0 | all-reduce | flops 2048 | bytes 16384 | tf_op jit(solution)/shard_map/psum | solution.py:38
  95.3 0.0 copy-done
  95.3 0.0 copy-done.4
  95.3 6.3 %convolution_convert_fusion = bf16[1024,2048]{1,0:T(8,128)(2,1)} fusion(bf16[512,2048]{1,0:T(8,128)(2,1)S(1)} %copy-done, f32[1024,512]{1,0:T(8,128)} %get-tuple-element.6, f32[512]{0:T(512)S(1)} %copy-done.4, f32[512]{0:T(512)S(1)} %copy-done.5, f32[1024]{0:T(1024)S(1)} %get-tuple-element.39, f32[1024]{0:T(1024)S(1)} %get-tuple-element.38), kind=kOutput, calls=%fused_computation.39 | convolution fusion | flops 2154299392 | bytes 8400896 | tf_op jit(solution)/shard_map/dot_general | solution.py:44
  101.6 0.0 reduce-scatter.3.cloned.1.call-update
  101.6 3.5 %all-gather.5.cloned.1.call-done = bf16[128,8,2048]{2,1,0:T(8,128)(2,1)} async-done(((bf16[32,8,2048]{2,1,0:T(8,128)(2,1)}), bf16[128,8,2048]{2,1,0:T(8,128)(2,1)}) %all-gather.5.cloned.1.call-update) | async-done | bytes 4194320 | tf_op jit(solution)/shard_map/all_gather | solution.py:72
  105.1 6.6 %fusion.2 = f32[1024,512]{1,0:T(8,128)} fusion(bf16[128,8,2048]{2,1,0:T(8,128)(2,1)} %all-gather.5.cloned.1.call-done, bf16[1,2048,512]{2,1,0:T(8,128)(2,1)} %param.21), kind=kOutput, calls=%fused_computation.34 | convolution fusion | flops 2147483648 | bytes 8388608 | tf_op jit(solution)/shard_map/dot_general | solution.py:74
  111.7 11.5 %convert_bitcast_fusion = bf16[128,8,2048]{2,1,0:T(8,128)(2,1)} fusion(bf16[1,512,2048]{2,1,0:T(8,128)(2,1)} %param.23, f32[1024,512]{1,0:T(8,128)} %fusion.2, bf16[1,2048,512]{2,1,0:T(8,128)(2,1)} %param.22, bf16[128,8,2048]{2,1,0:T(8,128)(2,1)} %all-gather.5.cloned.1.call-done), kind=kOutput, calls=%fused_computation.38 | convolution fusion | flops 4300210176 | bytes 14680064 | tf_op jit(solution)/shard_map/dot_general | solution.py:79
  123.2 6.4 %copy.24 = bf16[128,8,2048]{2,0,1:T(8,128)(2,1)} copy(bf16[128,8,2048]{2,1,0:T(8,128)(2,1)} %convert_bitcast_fusion) | data formatting | bytes 8388608 | tf_op jit(solution)/shard_map/reshape | solution.py:81
  129.6 5.4 %all-to-all-start.1 = ((bf16[128,8,2048]{2,0,1:T(8,128)(2,1)}), bf16[128,8,2048]{2,0,1:T(8,128)(2,1)}, u32[]{:S(2)}, u32[]{:S(2)}) async-start(bf16[128,8,2048]{2,0,1:T(8,128)(2,1)} %copy.24), calls=%async_computation.2 | async-start | bytes 8388608 | tf_op jit(solution)/shard_map/all_to_all | solution.py:80
  135.1 0.3 reduce-scatter.5.cloned.1.call-start
  135.3 0.1 copy.26
  135.5 93.3 %all-to-all-done.1 = bf16[128,8,2048]{2,0,1:T(8,128)(2,1)} async-done(((bf16[128,8,2048]{2,0,1:T(8,128)(2,1)}), bf16[128,8,2048]{2,0,1:T(8,128)(2,1)}, u32[]{:S(2)}, u32[]{:S(2)}) %all-to-all-start.1) | async-done | bytes 4194336 | tf_op jit(solution)/shard_map/all_to_all | solution.py:80
  228.8 6.5 %copy.29 = bf16[128,8,2048]{2,1,0:T(8,128)(2,1)} copy(bf16[128,8,2048]{2,0,1:T(8,128)(2,1)} %all-to-all-done.1) | data formatting | bytes 8388608 | tf_op jit(solution)/shard_map/all_to_all | solution.py:80
  235.2 8.0 %gather_fusion.1 = bf16[512,2048]{1,0:T(8,128)(2,1)} fusion(bf16[1024,2048]{1,0:T(8,128)(2,1)} %bitcast.70, s32[1024]{0:T(1024)S(1)} %pad_clamp_fusion), kind=kCustom, calls=%fused_computation.1 | custom fusion | bytes 4196352 | tf_op jit(solution)/shard_map/gather | solution.py:87
  243.2 5.4 %reshape.95 = f32[256,2,2048]{2,1,0:T(2,128)} reshape(bf16[512,2048]{1,0:T(8,128)(2,1)} %gather_fusion.1) | data formatting | bytes 6291456 | tf_op jit(solution)/shard_map/convert_element_type | solution.py:87
  248.6 10.0 %multiply_reduce_fusion = bf16[256,2048]{1,0:T(8,128)(2,1)} fusion(f32[256,2,2048]{2,1,0:T(2,128)} %reshape.95, f32[256,2]{1,0:T(8,128)S(1)} %copy.26), kind=kLoop, calls=%fused_computation.37 | loop fusion | flops 1572864 | bytes 5244928 | tf_op jit(solution)/shard_map/reduce_sum | solution.py:88
  258.6 0.0 reduce-scatter.5.cloned.1.call-update
  258.6 0.0 reduce-scatter.3.cloned.1.call-done
  258.6 23.0 %reduce-scatter.5.cloned.1.call-done = bf16[64,2048]{1,0:T(8,128)(2,1)} async-done(((bf16[256,2048]{1,0:T(8,128)(2,1)}), bf16[64,2048]{1,0:T(8,128)(2,1)}) %reduce-scatter.5.cloned.1.call-update) | async-done | bytes 262160 | tf_op jit(solution)/shard_map/reduce_scatter | solution.py:91
  (20 shorter events, 0.2 us)
Async XLA Ops:
  7.2 88.1 %copy-start = (bf16[512,2048]{1,0:T(8,128)(2,1)S(1)}, bf16[512,2048]{1,0:T(8,128)(2,1)}, u32[]{:S(2)}) copy-start(bf16[512,2048]{1,0:T(8,128)(2,1)} %param.16) | copy-start | bytes 6291460
  7.2 22.7 %all-gather.3.cloned.1.call-start = ((), (), s32[]{:S(2)}) async-start(), calls=%async_computation.5 | async-start | bytes 1310720 | tf_op jit(solution)/shard_map/all_gather | solution.py:55
  10.3 94.8 %all-gather.5.cloned.1.call-start = ((), (), s32[]{:S(2)}) async-start(), calls=%async_computation.6 | async-start | bytes 5242880 | tf_op jit(solution)/shard_map/all_gather | solution.py:72
  70.5 1.6 copy-start.1
  70.5 5.0 %copy-start.2 = (bf16[31,512]{1,0:T(8,128)(2,1)S(1)}, bf16[31,512]{1,0:T(8,128)(2,1)}, u32[]{:S(2)}) copy-start(bf16[31,512]{1,0:T(8,128)(2,1)} %param.13) | copy-start | bytes 95236
  72.1 23.2 %copy-start.4 = (f32[512]{0:T(512)S(1)}, f32[512]{0:T(512)}, u32[]{:S(2)}) copy-start(f32[512]{0:T(512)} %param.15) | copy-start | bytes 6148
  72.1 23.2 %copy-start.5 = (f32[512]{0:T(512)S(1)}, f32[512]{0:T(512)}, u32[]{:S(2)}) copy-start(f32[512]{0:T(512)} %param.14) | copy-start | bytes 6148
  72.1 186.5 %reduce-scatter.3.cloned.1.call-start = ((), (), s32[]{:S(2)}) async-start(), calls=%async_computation.4 | async-start | bytes 5242880 | tf_op jit(solution)/shard_map/reduce_scatter | solution.py:43
  72.2 5.0 %collective-permute-start = (bf16[30,512]{1,0:T(8,128)(2,1)S(1)}, bf16[30,512]{1,0:T(8,128)(2,1)S(1)}, u32[]{:S(2)}, u32[]{:S(2)}) collective-permute-start(bf16[30,512]{1,0:T(8,128)(2,1)S(1)} %slice.192), channel_id=1, source_target_pairs={{0,4},{4,8},{8,12},{12,16},{16,20},{20,24},{24,28},{1,5},{5,9},{9,... | collective-permute-start | bytes 92168 | tf_op jit(solution)/shard_map/ppermute | solution.py:10
  129.6 5.7 %copy-start.3 = (f32[256,2]{0,1:T(2,128)S(1)}, f32[256,2]{0,1:T(2,128)}, u32[]{:S(2)}) copy-start(f32[256,2]{0,1:T(2,128)} %param.20) | copy-start | bytes 6148
  129.6 99.1 %all-to-all-start.1 = ((bf16[128,8,2048]{2,0,1:T(8,128)(2,1)}), bf16[128,8,2048]{2,0,1:T(8,128)(2,1)}, u32[]{:S(2)}, u32[]{:S(2)}) async-start(bf16[128,8,2048]{2,0,1:T(8,128)(2,1)} %copy.24), calls=%async_computation.2 | async-start | bytes 8388608 | tf_op jit(solution)/shard_map/all_to_all | solution.py:80
  135.1 146.6 %reduce-scatter.5.cloned.1.call-start = ((), (), s32[]{:S(2)}) async-start(), calls=%async_computation.7 | async-start | bytes 1310720 | tf_op jit(solution)/shard_map/reduce_scatter | solution.py:91
Sparse Core Ops, SparseCore 0:
  10.4 19.4 all-gather.2
  72.2 32.8 all-gather.4
  108.2 44.5 reduce-scatter.2
  258.7 22.9 reduce-scatter.4
where the time goes:
time: 289 us; the launch traced here: 288 us
  waiting for transfers between devices  136 us (47%)
  local copies, waits for them, and re-layouts  41.2 us (14%)
  blocking collectives  38.4 us (13%)
  other arithmetic  25.5 us (9%)
  matrix products  24.4 us (8%)
  between operations  14 us (5%)
  starting transfers between devices  9.18 us (3%)
    all_to_all x1, waiting for transfers between devices, local(): lax.all_to_all(pieces.reshape(capacity, ep_count, model_width), 'ep', spl...  93.3 us
    all_to_all x1, blocking collectives, local(): lax.all_to_all(own_slots, 'ep', split_axis=1, concat_axis=1, tiled=True)  31.4 us
    reduce_scatter x1, waiting for transfers between devices, local(): lax.psum_scatter(combined.astype(jnp.bfloat16), 'tp', scatter_dimension=0...  23 us
    all_gather x1, waiting for transfers between devices, local(): group = lax.all_gather(normed, 'tp', axis=0, tiled=True)  14.3 us
    dot_general x1, matrix products, local(): jnp.dot(hidden, down_proj[0], preferred_element_type=jnp.float32)  11.5 us
    reduce_sum x1, other arithmetic, local(): jnp.sum(mixed, axis=1)  11.2 us
    reduce_sum x1, other arithmetic, local(): jnp.sum((picked * weights_flat[:, None]).reshape(group_rows, top_count, m...  9.96 us
    gather x1, local copies, waits for them, and re-layouts, local(): picked = returned.reshape(-1, model_width)[targets].astype(jnp.float32)  7.95 us
  transfers between devices with their start and end apart: 6, of which 5 were waited for; matrix products, arithmetic and copies ran while one was open for 27% of the time, Pallas kernels for 0%

commit v1 on v0

--- a/solution.py
+++ b/solution.py
@@ -56,37 +56,41 @@
     group_rows, top_count = routes.shape
     model_width = group.shape[1]
     capacity = 2 * top_count * group_rows // ep_count
-    expert_ids = routes.reshape(-1)
-    onehot = (expert_ids[:, None] == jnp.arange(ep_count, dtype=jnp.int32)[None, :]).astype(
+    share = capacity // tp_count
+    experts = jnp.arange(ep_count, dtype=jnp.int32)
+    named = routes.T[None, :, :] == experts[:, None, None]
+    hit = jnp.any(named, axis=1)
+    weight = jnp.sum(jnp.where(named, route_weights.T[None, :, :], 0.0), axis=1)
+    tokens = jnp.arange(group_rows, dtype=jnp.int32)
+    before = (tokens[:, None] < tokens[None, :]).astype(jnp.bfloat16)
+    rank = jnp.dot(hit.astype(jnp.bfloat16), before, preferred_element_type=jnp.float32).astype(
         jnp.int32
     )
-    ranks = jnp.sum((jnp.cumsum(onehot, axis=0) - onehot) * onehot, axis=1)
-    targets = ranks * ep_count + expert_ids
-    owners = jnp.arange(group_rows * top_count, dtype=jnp.int32) // top_count
-    table = jnp.full((capacity * ep_count,), group_rows, jnp.int32).at[targets].set(owners)
-    extended = jnp.concatenate([group, jnp.zeros((1, model_width), jnp.bfloat16)], axis=0)
-    outgoing = extended[table].reshape(capacity, ep_count, model_width)
-    share = capacity // tp_count
-    own_slots = lax.dynamic_slice_in_dim(outgoing, lax.axis_index("tp") * share, share, 0)
-    landed = lax.all_to_all(own_slots, "ep", split_axis=1, concat_axis=1, tiled=True)
-    arrived = lax.all_gather(landed, "tp", axis=0, tiled=True)
-    incoming = arrived.reshape(capacity * ep_count, model_width)
+    first = lax.axis_index("tp") * share
+    slots = first + jnp.arange(share, dtype=jnp.int32)
+    held = hit[:, None, :] & (rank[:, None, :] == slots[None, :, None])
+    pick = held.astype(jnp.bfloat16).reshape(ep_count * share, group_rows)
+    scale = (
+        jnp.where(held, weight[:, None, :], 0.0)
+        .astype(jnp.bfloat16)
+        .reshape(ep_count * share, group_rows)
+    )
+    outgoing = jnp.dot(pick, group, preferred_element_type=jnp.float32).astype(jnp.bfloat16)
+    landed = lax.all_to_all(
+        outgoing.reshape(ep_count, share, model_width), "ep", split_axis=0, concat_axis=0, tiled=True
+    ).reshape(ep_count * share, model_width)
+    incoming = lax.all_gather(landed, "tp", axis=0, tiled=True)
     gated = jax.nn.silu(jnp.dot(incoming, gate_proj[0], preferred_element_type=jnp.float32))
     hidden = (gated * jnp.dot(incoming, up_proj[0], preferred_element_type=jnp.float32)).astype(
         jnp.bfloat16
     )
-    weights_flat = route_weights.reshape(-1)
     pieces = jnp.dot(hidden, down_proj[0], preferred_element_type=jnp.float32).astype(jnp.bfloat16)
+    summed = lax.psum_scatter(pieces, "tp", scatter_dimension=0, tiled=True)
     returned = lax.all_to_all(
-        pieces.reshape(capacity, ep_count, model_width),
-        "ep",
-        split_axis=1,
-        concat_axis=1,
-        tiled=True,
-    )
-    picked = returned.reshape(-1, model_width)[targets].astype(jnp.float32)
-    combined = jnp.sum(
-        (picked * weights_flat[:, None]).reshape(group_rows, top_count, model_width), axis=1
+        summed.reshape(ep_count, share, model_width), "ep", split_axis=0, concat_axis=0, tiled=True
+    ).reshape(ep_count * share, model_width)
+    combined = lax.dot_general(
+        scale, returned, (((0,), (0,)), ((), ())), preferred_element_type=jnp.float32
     )
     moe_out = lax.psum_scatter(combined.astype(jnp.bfloat16), "tp", scatter_dimension=0, tiled=True)
     return (conv_out, moe_out)

time: 289 us -> 240 us (0.83)
  local copies, waits for them, and re-layouts: 41.2 us -> 1.31 us
  other arithmetic: 25.5 us -> 15.1 us
    all_to_all x1, waiting for transfers between devices: 93.3 us -> 25.6 us  [local(): lax.all_to_all(summed.reshape(ep_count, share, model_width), 'ep', split_...]
    all_gather x1, waiting for transfers between devices: 3.46 us -> 32.7 us  [local(): incoming = lax.all_gather(landed, 'tp', axis=0, tiled=True)]
    reduce_scatter x1, waiting for transfers between devices: 0.02 us -> 14.9 us  [local(): lax.psum_scatter(jnp.dot(activated, conv_proj, preferred_element_type=jnp...]
    reduce_scatter x0 -> x1, waiting for transfers between devices: none -> 14 us  [local(): summed = lax.psum_scatter(pieces, 'tp', scatter_dimension=0, tiled=True)]
    gather x2 -> x0, local copies, waits for them, and re-layouts: 14 us -> none  [the longest x1 7.95 us: local(): picked = returned.reshape(-1, model_width)[targets].astype(jnp.float32)]
    reduce_sum x2 -> x1, other arithmetic: 10 us -> 0.01 us  [local(): weight = jnp.sum(jnp.where(named, route_weights.T[None, :, :], 0.0), axis=1)]
    all_to_all x2 -> x0, local copies, waits for them, and re-layouts: 8.02 us -> none  [the longest x1 6.46 us: local(): lax.all_to_all(pieces.reshape(capacity, ep_count, model_width), 'ep', spl...]
    reshape x2 -> x0, local copies, waits for them, and re-layouts: 6.58 us -> none  [the longest x1 6.44 us: local(): pieces.reshape(capacity, ep_count, model_width)]
  transfers between devices with their start and end apart: 6 -> 7, of which waited for: 5 -> 7; matrix products, arithmetic and copies ran while one was open for 27% -> 9% of each run, Pallas kernels for 0% -> 0%
where the time goes in v1:
time: 240 us; the launch traced here: 239 us
  waiting for transfers between devices  135 us (56%)
  blocking collectives  38.2 us (16%)
  matrix products  26.9 us (11%)
  other arithmetic  15.1 us (6%)
  between operations  14 us (6%)
  starting transfers between devices  9.07 us (4%)
    all_gather x1, waiting for transfers between devices, local(): incoming = lax.all_gather(landed, 'tp', axis=0, tiled=True)  32.7 us
    all_to_all x1, blocking collectives, local(): lax.all_to_all(outgoing.reshape(ep_count, share, model_width), 'ep', spli...  31.5 us
    reduce_scatter x1, waiting for transfers between devices, local(): lax.psum_scatter(combined.astype(jnp.bfloat16), 'tp', scatter_dimension=0...  27.8 us
    all_to_all x1, waiting for transfers between devices, local(): lax.all_to_all(summed.reshape(ep_count, share, model_width), 'ep', split_...  25.6 us
    all_gather x1, waiting for transfers between devices, local(): group = lax.all_gather(normed, 'tp', axis=0, tiled=True)  18.5 us
    reduce_scatter x1, waiting for transfers between devices, local(): lax.psum_scatter(jnp.dot(activated, conv_proj, preferred_element_type=jnp...  14.9 us
    reduce_scatter x1, waiting for transfers between devices, local(): summed = lax.psum_scatter(pieces, 'tp', scatter_dimension=0, tiled=True)  14 us
    reduce_sum x1, other arithmetic, local(): jnp.sum(mixed, axis=1)  11.2 us
  transfers between devices with their start and end apart: 7, of which 7 were waited for; matrix products, arithmetic and copies ran while one was open for 9% of the time, Pallas kernels for 0%

profile of v1, /device:TPU:0, one launch (start us, length us, event | category | flops | bytes accessed | tf_op | source)
XLA Modules:
  0.0 239.4 jit_solution(10050856176639902274)
XLA Ops:
  7.2 0.0 copy-start
  7.2 0.0 all-gather.3.cloned.1.call-start
  7.2 1.2 fusion.44
  8.5 1.8 fusion.46
  10.3 0.0 all-gather.3.cloned.1.call-update
  10.3 0.0 all-gather.5.cloned.1.call-start
  10.4 0.1 eq.45
  10.5 0.7 fusion.53
  11.1 0.1 convolution_convert_fusion.3
  11.3 0.1 fusion.47
  11.4 18.5 %all-gather.3.cloned.1.call-done = bf16[256,2048]{1,0:T(8,128)(2,1)} async-done(((bf16[64,2048]{1,0:T(8,128)(2,1)}), bf16[256,2048]{1,0:T(8,128)(2,1)}) %all-gather.3.cloned.1.call-update) | async-done | bytes 1048592 | tf_op jit(solution)/shard_map/all_gather | solution.py:55
  29.9 1.7 convolution_convert_fusion.2
  31.6 31.5 %all_to_all.10 = bf16[8,32,2048]{2,1,0:T(8,128)(2,1)} all-to-all(bf16[8,32,2048]{2,1,0:T(8,128)(2,1)S(1)} %bitcast.67), channel_id=1, replica_groups=mesh['ep'=8,'tp'=4] {'ep'}, dimensions={0} | all-to-all | bytes 2097152 | tf_op jit(solution)/shard_map/all_to_all | solution.py:79
  63.1 0.0 all-gather.5.cloned.1.call-update
  63.1 0.0 reduce-scatter.6.cloned.1.call-start
  63.2 32.7 %all-gather.5.cloned.1.call-done = bf16[1024,2048]{1,0:T(8,128)(2,1)} async-done(((bf16[256,2048]{1,0:T(8,128)(2,1)}), bf16[1024,2048]{1,0:T(8,128)(2,1)}) %all-gather.5.cloned.1.call-update) | async-done | bytes 4194320 | tf_op jit(solution)/shard_map/all_gather | solution.py:82
  95.8 6.5 %fusion.2 = f32[1024,512]{1,0:T(8,128)} fusion(bf16[1024,2048]{1,0:T(8,128)(2,1)} %all-gather.5.cloned.1.call-done, bf16[1,2048,512]{2,1,0:T(8,128)(2,1)} %param.22), kind=kOutput, calls=%fused_computation.35 | convolution fusion | flops 2147483648 | bytes 8388608 | tf_op jit(solution)/shard_map/dot_general | solution.py:84
  102.4 0.0 copy-done
  102.4 10.1 %convolution_convert_fusion = bf16[1024,2048]{1,0:T(8,128)(2,1)} fusion(bf16[1,512,2048]{2,1,0:T(8,128)(2,1)S(1)} %copy-done, f32[1024,512]{1,0:T(8,128)} %fusion.2, bf16[1024,2048]{1,0:T(8,128)(2,1)} %all-gather.5.cloned.1.call-done, bf16[1,2048,512]{2,1,0:T(8,128)(2,1)} %param.21), kind=kOutput, calls=%fused_computation.29 | convolution fusion | flops 4300210176 | bytes 14680064 | tf_op jit(solution)/shard_map/dot_general | solution.py:87
  112.5 0.0 copy-start.1
  112.5 0.0 copy-start.2
  112.5 0.0 reduce-scatter.6.cloned.1.call-update
  112.5 0.0 copy-start.5
  112.5 0.0 copy-start.6
  112.5 0.0 reduce-scatter.4.cloned.1.call-start
  112.6 1.1 copy-done.1
  113.7 3.4 %collective-permute-start = (bf16[30,512]{1,0:T(8,128)(2,1)S(1)}, bf16[30,512]{1,0:T(8,128)(2,1)S(1)}, u32[]{:S(2)}, u32[]{:S(2)}) collective-permute-start(bf16[30,512]{1,0:T(8,128)(2,1)S(1)} %slice.186), channel_id=1, source_target_pairs={{0,4},{4,8},{8,12},{12,16},{16,20},{20,24},{24,28},{1,5},{5,9},{9,... | collective-permute-start | bytes 92168 | tf_op jit(solution)/shard_map/ppermute | solution.py:10
  117.1 0.0 copy-done.2
  117.2 1.5 collective-permute-done
  118.7 11.2 %fusion.57 = (f32[1024]{0:T(1024)S(1)}, f32[1024]{0:T(1024)S(1)}, f32[1024,512]{1,0:T(8,128)}) fusion(f32[512]{0:T(512)S(1)} %bitcast.101, bf16[1024,512]{1,0:T(8,128)(2,1)S(1)} %copy-done.1, f32[512]{0:T(512)S(1)} %bitcast.100, bf16[30,512]{1,0:T(8,128)(2,1)S(1)} %collective-permute-done, f32[512]{0:T(512)S(1)} %bitcast.99, f32[512]{0:T(512)S(1)} %bitcast.98, ...), kind=kLoop, calls=%fused_computation.107 | loop fusion | flops 96991232 | bytes 3248128 | tf_op jit(solution)/shard_map/reduce_sum | solution.py:38
  129.8 6.6 %all-reduce = (f32[1024]{0:T(1024)S(1)}, f32[1024]{0:T(1024)S(1)}) all-reduce(f32[1024]{0:T(1024)S(1)} %get-tuple-element.3, f32[1024]{0:T(1024)S(1)} %get-tuple-element.2), channel_id=1, replica_groups=mesh['ep'=8,'tp'=4] {'tp'}, use_global_device_ids=true, to_apply=%region_3.0 | all-reduce | flops 2048 | bytes 16384 | tf_op jit(solution)/shard_map/psum | solution.py:38
  136.5 0.0 copy-done.5
  136.5 0.0 copy-done.6
  136.5 6.9 %convolution_convert_fusion.1 = bf16[1024,2048]{1,0:T(8,128)(2,1)} fusion(bf16[512,2048]{1,0:T(8,128)(2,1)} %param.16, f32[1024,512]{1,0:T(8,128)} %get-tuple-element.6, f32[512]{0:T(512)S(1)} %copy-done.5, f32[512]{0:T(512)S(1)} %copy-done.6, f32[1024]{0:T(1024)S(1)} %get-tuple-element.39, f32[1024]{0:T(1024)S(1)} %get-tuple-element.38), kind=kOutput, calls=%fused_computation.30 | convolution fusion | flops 2154299392 | bytes 8400896 | tf_op jit(solution)/shard_map/dot_general | solution.py:44
  143.4 0.0 reduce-scatter.4.cloned.1.call-update
  143.5 0.0 copy-start.3
  143.5 0.0 copy-start.4
  143.5 14.0 %reduce-scatter.6.cloned.1.call-done = bf16[256,2048]{1,0:T(8,128)(2,1)} async-done(((bf16[1024,2048]{1,0:T(8,128)(2,1)}), bf16[256,2048]{1,0:T(8,128)(2,1)}) %reduce-scatter.6.cloned.1.call-update) | async-done | bytes 1048592 | tf_op jit(solution)/shard_map/reduce_scatter | solution.py:88
  157.5 5.5 %all-to-all-start.1 = ((bf16[8,32,2048]{2,1,0:T(8,128)(2,1)}), bf16[8,32,2048]{2,1,0:T(8,128)(2,1)S(1)}, u32[]{:S(2)}, u32[]{:S(2)}) async-start(bf16[8,32,2048]{2,1,0:T(8,128)(2,1)} %bitcast.68), calls=%async_computation.3 | async-start | bytes 2097152 | tf_op jit(solution)/shard_map/all_to_all | solution.py:89
  163.0 0.0 reduce-scatter.8.cloned.1.call-start
  163.1 0.0 copy-done.3
  163.1 0.0 copy-done.4
  163.1 25.6 %all-to-all-done.1 = bf16[8,32,2048]{2,1,0:T(8,128)(2,1)S(1)} async-done(((bf16[8,32,2048]{2,1,0:T(8,128)(2,1)}), bf16[8,32,2048]{2,1,0:T(8,128)(2,1)S(1)}, u32[]{:S(2)}, u32[]{:S(2)}) %all-to-all-start.1) | async-done | bytes 1048608 | tf_op jit(solution)/shard_map/all_to_all | solution.py:89
  188.7 1.5 fusion
  190.2 0.0 reduce-scatter.8.cloned.1.call-update
  190.2 14.9 %reduce-scatter.4.cloned.1.call-done = bf16[256,2048]{1,0:T(8,128)(2,1)} async-done(((bf16[1024,2048]{1,0:T(8,128)(2,1)}), bf16[256,2048]{1,0:T(8,128)(2,1)}) %reduce-scatter.4.cloned.1.call-update) | async-done | bytes 1048592 | tf_op jit(solution)/shard_map/reduce_scatter | solution.py:43
  205.1 27.8 %reduce-scatter.8.cloned.1.call-done = bf16[64,2048]{1,0:T(8,128)(2,1)} async-done(((bf16[256,2048]{1,0:T(8,128)(2,1)}), bf16[64,2048]{1,0:T(8,128)(2,1)}) %reduce-scatter.8.cloned.1.call-update) | async-done | bytes 262160 | tf_op jit(solution)/shard_map/reduce_scatter | solution.py:95
  (8 shorter events, 0.1 us)
Async XLA Ops:
  7.2 95.2 %copy-start = (bf16[1,512,2048]{2,1,0:T(8,128)(2,1)S(1)}, bf16[1,512,2048]{2,1,0:T(8,128)(2,1)}, u32[]{:S(2)}) copy-start(bf16[1,512,2048]{2,1,0:T(8,128)(2,1)} %param.23) | copy-start | bytes 6291460
  7.2 22.7 %all-gather.3.cloned.1.call-start = ((), (), s32[]{:S(2)}) async-start(), calls=%async_computation.6 | async-start | bytes 1310720 | tf_op jit(solution)/shard_map/all_gather | solution.py:55
  10.3 85.5 %all-gather.5.cloned.1.call-start = ((), (), s32[]{:S(2)}) async-start(), calls=%async_computation.7 | async-start | bytes 5242880 | tf_op jit(solution)/shard_map/all_gather | solution.py:82
  63.1 94.4 %reduce-scatter.6.cloned.1.call-start = ((), (), s32[]{:S(2)}) async-start(), calls=%async_computation.8 | async-start | bytes 5242880 | tf_op jit(solution)/shard_map/reduce_scatter | solution.py:88
  112.5 1.2 copy-start.1
  112.5 4.6 %copy-start.2 = (bf16[31,512]{1,0:T(8,128)(2,1)S(1)}, bf16[31,512]{1,0:T(8,128)(2,1)}, u32[]{:S(2)}) copy-start(bf16[31,512]{1,0:T(8,128)(2,1)} %param.13) | copy-start | bytes 95236
  112.5 24.0 %copy-start.5 = (f32[512]{0:T(512)S(1)}, f32[512]{0:T(512)}, u32[]{:S(2)}) copy-start(f32[512]{0:T(512)} %param.15) | copy-start | bytes 6148
  112.5 24.0 %copy-start.6 = (f32[512]{0:T(512)S(1)}, f32[512]{0:T(512)}, u32[]{:S(2)}) copy-start(f32[512]{0:T(512)} %param.14) | copy-start | bytes 6148
  112.5 92.6 %reduce-scatter.4.cloned.1.call-start = ((), (), s32[]{:S(2)}) async-start(), calls=%async_computation.5 | async-start | bytes 5242880 | tf_op jit(solution)/shard_map/reduce_scatter | solution.py:43
  113.7 5.0 %collective-permute-start = (bf16[30,512]{1,0:T(8,128)(2,1)S(1)}, bf16[30,512]{1,0:T(8,128)(2,1)S(1)}, u32[]{:S(2)}, u32[]{:S(2)}) collective-permute-start(bf16[30,512]{1,0:T(8,128)(2,1)S(1)} %slice.186), channel_id=1, source_target_pairs={{0,4},{4,8},{8,12},{12,16},{16,20},{20,24},{24,28},{1,5},{5,9},{9,... | collective-permute-start | bytes 92168 | tf_op jit(solution)/shard_map/ppermute | solution.py:10
  143.5 19.6 %copy-start.3 = (s32[256,2]{0,1:T(2,128)S(1)}, s32[256,2]{0,1:T(2,128)}, u32[]{:S(2)}) copy-start(s32[256,2]{0,1:T(2,128)} %param.19) | copy-start | bytes 6148
  143.5 19.6 %copy-start.4 = (f32[256,2]{0,1:T(2,128)S(1)}, f32[256,2]{0,1:T(2,128)}, u32[]{:S(2)}) copy-start(f32[256,2]{0,1:T(2,128)} %param.20) | copy-start | bytes 6148
  157.5 31.2 %all-to-all-start.1 = ((bf16[8,32,2048]{2,1,0:T(8,128)(2,1)}), bf16[8,32,2048]{2,1,0:T(8,128)(2,1)S(1)}, u32[]{:S(2)}, u32[]{:S(2)}) async-start(bf16[8,32,2048]{2,1,0:T(8,128)(2,1)} %bitcast.68), calls=%async_computation.3 | async-start | bytes 2097152 | tf_op jit(solution)/shard_map/all_to_all | solution.py:89
  163.0 69.9 %reduce-scatter.8.cloned.1.call-start = ((), (), s32[]{:S(2)}) async-start(), calls=%async_computation.9 | async-start | bytes 1310720 | tf_op jit(solution)/shard_map/reduce_scatter | solution.py:95
Sparse Core Ops, SparseCore 0:
  10.4 19.4 all-gather.2
  63.2 32.5 all-gather.4
  112.6 44.8 reduce-scatter.5
  160.5 44.5 reduce-scatter.3
  208.0 24.8 reduce-scatter.7

commit v2 on v1

--- a/solution.py
+++ b/solution.py
@@ -1,7 +1,326 @@
+import functools
+
 import jax
 import jax.numpy as jnp
 from jax import lax
+from jax.experimental import pallas as pl
+from jax.experimental.pallas import tpu as pltpu
 from jax.sharding import PartitionSpec as P
+
+MESH = pl.DeviceIdType.MESH
+
+
+def hop_order(ep_count):
+    half = ep_count // 2
+    order = [0, half]
+    for near in range(1, half):
+        order += [half - near, half + near]
+    return order
+
+
+def exchange(
+    normed, pick, scale, partial, gate_hbm, up_hbm, down_hbm,
+    conv_out, moe_out,
+    gate, up, down, group, outgoing, arrived, pieces, from_core, to_y, from_y, to_ep, returned,
+    conv_core, conv_to_y, conv_from_y, combined, last_core, last_to_y, last_from_y,
+    weight_sem, ag_send, ag_recv, ep_send, ep_recv, fan_send, fan_recv,
+    core_send, core_recv, y_send, y_recv, back_send, back_recv,
+    conv_send, conv_recv, last_send, last_recv,
+    *, ep_count, share,
+):
+    order = hop_order(ep_count)
+    me_ep, me = lax.axis_index("ep"), lax.axis_index("tp")
+    core = me + 1 - 2 * (me % 2)
+    over = (me + 2) % 4
+    far = (core + 2) % 4
+    rows, width = normed.shape
+    f32, bf16 = jnp.float32, jnp.bfloat16
+
+    def remote(src, dst, send, recv, where):
+        return pltpu.make_async_remote_copy(
+            src_ref=src, dst_ref=dst, send_sem=send, recv_sem=recv, device_id=where,
+            device_id_type=MESH,
+        )
+
+    def block(ref, index, size):
+        return ref.at[pl.ds(pl.multiple_of(index * size, size), size)]
+
+    loads = [
+        pltpu.make_async_copy(src, dst, weight_sem.at[i])
+        for i, (src, dst) in enumerate(((gate_hbm, gate), (up_hbm, up), (down_hbm, down)))
+    ]
+    for load in loads:
+        load.start()
+    barrier = pltpu.get_barrier_semaphore()
+    pl.semaphore_signal(barrier, inc=1, device_id={"tp": core}, device_id_type=MESH)
+    pl.semaphore_signal(barrier, inc=1, device_id={"tp": over}, device_id_type=MESH)
+    for d in range(1, ep_count):
+        pl.semaphore_signal(
+            barrier, inc=1, device_id={"ep": (me_ep + d) % ep_count}, device_id_type=MESH
+        )
+    pl.semaphore_wait(barrier, ep_count + 1)
+
+    sent = []
+
+    ag = [
+        remote(normed, block(group, me, rows), ag_send.at[0], ag_recv.at[0], {"tp": over}),
+        remote(normed, block(group, me, rows), ag_send.at[1], ag_recv.at[1], {"tp": core}),
+        remote(block(group, over, rows), block(group, over, rows), ag_send.at[2], ag_recv.at[2], {"tp": core}),
+    ]
+    ag[0].start()
+    ag[1].start()
+    group[pl.ds(pl.multiple_of(me * rows, rows), rows), :] = normed[...]
+    span = partial.shape[0] // 4
+    conv = [
+        remote(
+            block(partial, core if n == 0 else far, span), conv_core.at[n],
+            conv_send.at[n], conv_recv.at[n], {"tp": core},
+        )
+        for n in range(2)
+    ]
+    ag[0].wait_recv()
+    ag[2].start()
+    conv[1].start()
+    conv[0].start()
+    ag[1].wait_recv()
+    ag[2].wait_recv()
+    sent += ag + conv
+
+    tile = 512
+    for n in range(0, width, tile):
+        part = jnp.dot(pick[...], group[:, n : n + tile], preferred_element_type=f32).astype(bf16)
+        outgoing[:, n : n + tile] = part
+        arrived[pl.ds(pl.multiple_of(me * share, share), share), n : n + tile] = part[:share]
+    ep = []
+    for s in range(1, ep_count):
+        ep.append(
+            remote(
+                outgoing.at[s * share : (s + 1) * share], block(arrived, s * 4 + me, share),
+                ep_send.at[s], ep_recv.at[s], {"ep": (me_ep + order[s]) % ep_count},
+            )
+        )
+        ep[-1].start()
+    sent += ep
+
+    def fan(kind, s):
+        quarter = over if kind == 2 else me
+        place = block(arrived, s * 4 + quarter, share)
+        return remote(
+            place, place, fan_send.at[kind, s], fan_recv.at[kind, s],
+            {"tp": over if kind == 0 else core},
+        )
+
+    fans = [[fan(kind, s) for s in range(ep_count)] for kind in range(3)]
+    for kind in range(3):
+        sent += fans[kind]
+
+    def relay(s):
+        fans[0][s].wait_recv()
+        fans[2][s].start()
+
+    def land(s):
+        if s > 0:
+            ep[s - 1].wait_recv()
+        fans[0][s].start()
+        fans[1][s].start()
+
+    conv_y = [
+        remote(conv_to_y.at[n], conv_from_y.at[n], conv_send.at[2 + n], conv_recv.at[2 + n], {"tp": over})
+        for n in range(4)
+    ]
+    sent += conv_y
+    piece_rows = span // 4
+
+    def conv_half():
+        conv[1].wait_recv()
+        for n in range(4):
+            at = pl.multiple_of(over * span + n * piece_rows, piece_rows)
+            conv_to_y[n] = (
+                partial[pl.ds(at, piece_rows), :].astype(f32)
+                + conv_core[1, n * piece_rows : (n + 1) * piece_rows, :].astype(f32)
+            ).astype(bf16)
+            conv_y[n].start()
+
+    chunk = 2 * 4 * share
+
+    def experts(c):
+        for s in (2 * c, 2 * c + 1):
+            fans[1][s].wait_recv()
+            fans[2][s].wait_recv()
+        here = slice(c * chunk, (c + 1) * chunk)
+        lines = arrived[here, :]
+        left = jnp.dot(lines, gate[...], preferred_element_type=f32)
+        right = jnp.dot(lines, up[...], preferred_element_type=f32)
+        hidden = (left / (1.0 + jnp.exp(-left)) * right).astype(bf16)
+        for n in range(0, width, tile):
+            pieces[here, n : n + tile] = jnp.dot(
+                hidden, down[:, n : n + tile], preferred_element_type=f32
+            ).astype(bf16)
+        for s in (2 * c, 2 * c + 1):
+            cores[s][1].start()
+            cores[s][0].start()
+
+    cores = [
+        [
+            remote(
+                block(pieces, s * 4 + (core if n == 0 else far), share), from_core.at[s, n],
+                core_send.at[s, n], core_recv.at[s, n], {"tp": core},
+            )
+            for n in range(2)
+        ]
+        for s in range(ep_count)
+    ]
+    ys = [
+        remote(to_y.at[s], from_y.at[s], y_send.at[s], y_recv.at[s], {"tp": over})
+        for s in range(ep_count)
+    ]
+    backs = [
+        remote(
+            to_ep.at[s], returned.at[s * share : (s + 1) * share], back_send.at[s], back_recv.at[s],
+            {"ep": (me_ep + ep_count - order[s]) % ep_count},
+        )
+        for s in range(1, ep_count)
+    ]
+    for s in range(ep_count):
+        sent += cores[s]
+    sent += ys + backs
+
+    def mine(s, quarter, n):
+        at = pl.multiple_of((s * 4 + quarter) * share, share)
+        return pieces[pl.ds(at, share), :].astype(f32) + from_core[s, n].astype(f32)
+
+    def across(c):
+        for s in (2 * c, 2 * c + 1):
+            cores[s][1].wait_recv()
+            to_y[s] = mine(s, over, 1).astype(bf16)
+            ys[s].start()
+
+    def back(c):
+        for s in (2 * c, 2 * c + 1):
+            cores[s][0].wait_recv()
+            ys[s].wait_recv()
+            total = (mine(s, me, 0) + from_y[s].astype(f32)).astype(bf16)
+            if s == 0:
+                returned[:share, :] = total
+            else:
+                to_ep[s] = total
+                backs[s - 1].start()
+
+    chunks = ep_count // 2
+    land(0)
+    for s in range(1, ep_count):
+        land(s)
+        if s >= 2:
+            relay(s - 2)
+        if s == 3:
+            for load in loads:
+                load.wait()
+        if s == 5:
+            experts(0)
+    experts(1)
+    across(0)
+    relay(ep_count - 2)
+    relay(ep_count - 1)
+    conv_half()
+    for c in range(2, chunks):
+        experts(c)
+        across(c - 1)
+        back(c - 2)
+    across(chunks - 1)
+    back(chunks - 2)
+    conv[0].wait_recv()
+    for n in range(4):
+        conv_y[n].wait_recv()
+        at = pl.multiple_of(me * span + n * piece_rows, piece_rows)
+        conv_out[n * piece_rows : (n + 1) * piece_rows, :] = (
+            partial[pl.ds(at, piece_rows), :].astype(f32)
+            + conv_core[0, n * piece_rows : (n + 1) * piece_rows, :].astype(f32)
+            + conv_from_y[n].astype(f32)
+        ).astype(bf16)
+    back(chunks - 1)
+
+    for r in backs:
+        r.wait_recv()
+    for n in range(0, width, tile):
+        combined[:, n : n + tile] = jnp.dot(
+            scale[...], returned[:, n : n + tile], preferred_element_type=f32
+        ).astype(bf16)
+    last = [
+        remote(
+            block(combined, core if n == 0 else far, rows), last_core.at[n],
+            last_send.at[n], last_recv.at[n], {"tp": core},
+        )
+        for n in range(2)
+    ]
+    last[1].start()
+    last[0].start()
+    last.append(remote(last_to_y, last_from_y, last_send.at[2], last_recv.at[2], {"tp": over}))
+
+    def own(quarter, n):
+        at = pl.multiple_of(quarter * rows, rows)
+        return combined[pl.ds(at, rows), :].astype(f32) + last_core[n].astype(f32)
+
+    last[1].wait_recv()
+    last_to_y[...] = own(over, 1).astype(bf16)
+    last[2].start()
+    last[0].wait_recv()
+    last[2].wait_recv()
+    moe_out[...] = (own(me, 0) + last_from_y[...].astype(f32)).astype(bf16)
+    sent += last
+    for r in sent:
+        r.wait_send()
+
+
+def run_exchange(normed, pick, scale, partial, gate, up, down, ep_count, share):
+    rows, width = normed.shape
+    hid = gate.shape[1]
+    span = partial.shape[0] // 4
+    bf16 = jnp.bfloat16
+    slots = ep_count * share
+    vmem, dma = pltpu.VMEM, pltpu.SemaphoreType.DMA
+    at_vmem, at_any = pl.BlockSpec(memory_space=pltpu.VMEM), pl.BlockSpec(memory_space=pl.ANY)
+    return pl.pallas_call(
+        functools.partial(exchange, ep_count=ep_count, share=share),
+        out_shape=(
+            jax.ShapeDtypeStruct((span, width), bf16),
+            jax.ShapeDtypeStruct((rows, width), bf16),
+        ),
+        in_specs=[at_vmem] * 4 + [at_any] * 3,
+        out_specs=(at_vmem, at_vmem),
+        scratch_shapes=[
+            vmem((width, hid), bf16),
+            vmem((width, hid), bf16),
+            vmem((hid, width), bf16),
+            vmem((4 * rows, width), bf16),
+            vmem((slots, width), bf16),
+            vmem((4 * slots, width), bf16),
+            vmem((4 * slots, width), bf16),
+            vmem((ep_count, 2, share, width), bf16),
+            vmem((ep_count, share, width), bf16),
+            vmem((ep_count, share, width), bf16),
+            vmem((ep_count, share, width), bf16),
+            vmem((slots, width), bf16),
+            vmem((2, span, width), bf16),
+            vmem((4, span // 4, width), bf16),
+            vmem((4, span // 4, width), bf16),
+            vmem((4 * rows, width), bf16),
+            vmem((2, rows, width), bf16),
+            vmem((rows, width), bf16),
+            vmem((rows, width), bf16),
+            dma((3,)),
+            dma((3,)), dma((3,)),
+            dma((ep_count,)), dma((ep_count,)),
+            dma((3, ep_count)), dma((3, ep_count)),
+            dma((ep_count, 2)), dma((ep_count, 2)),
+            dma((ep_count,)), dma((ep_count,)),
+            dma((ep_count,)), dma((ep_count,)),
+            dma((6,)), dma((6,)),
+            dma((3,)), dma((3,)),
+        ],
+        compiler_params=pltpu.CompilerParams(
+            collective_id=0, has_side_effects=True, vmem_limit_bytes=60 * 1024 * 1024
+        ),
+    )(normed, pick, scale, partial, gate, up, down)
 
 
 def shifted(value, axis, steps):
@@ -40,24 +359,23 @@
     spread = jnp.maximum(squares / full_width - center * center, 0.0)
     scaled = (mixed - center[:, None]) * lax.rsqrt(spread[:, None] + 1e-05) * norm_gain + norm_shift
     activated = jax.nn.silu(scaled).astype(jnp.bfloat16)
-    conv_out = lax.psum_scatter(
-        jnp.dot(activated, conv_proj, preferred_element_type=jnp.float32).astype(jnp.bfloat16),
-        "tp",
-        scatter_dimension=0,
-        tiled=True,
-    )
+    partial = jnp.dot(activated, conv_proj, preferred_element_type=jnp.float32).astype(jnp.bfloat16)
     moe_float = moe_input.astype(jnp.float32)
     normed = (
         moe_float
         * lax.rsqrt(jnp.mean(moe_float * moe_float, axis=1, keepdims=True) + 1e-06)
         * moe_gain
     ).astype(jnp.bfloat16)
-    group = lax.all_gather(normed, "tp", axis=0, tiled=True)
     group_rows, top_count = routes.shape
-    model_width = group.shape[1]
+    model_width = normed.shape[1]
     capacity = 2 * top_count * group_rows // ep_count
     share = capacity // tp_count
-    experts = jnp.arange(ep_count, dtype=jnp.int32)
+    direct = tp_count == 4 and share % 16 == 0 and ep_count % 2 == 0 and ep_count >= 8
+    if direct:
+        hops = jnp.array(hop_order(ep_count), jnp.int32)
+        experts = (lax.axis_index("ep") + hops) % ep_count
+    else:
+        experts = jnp.arange(ep_count, dtype=jnp.int32)
     named = routes.T[None, :, :] == experts[:, None, None]
     hit = jnp.any(named, axis=1)
     weight = jnp.sum(jnp.where(named, route_weights.T[None, :, :], 0.0), axis=1)
@@ -75,6 +393,12 @@
         .astype(jnp.bfloat16)
         .reshape(ep_count * share, group_rows)
     )
+    if direct:
+        return run_exchange(
+            normed, pick, scale.T, partial, gate_proj[0], up_proj[0], down_proj[0], ep_count, share
+        )
+    conv_out = lax.psum_scatter(partial, "tp", scatter_dimension=0, tiled=True)
+    group = lax.all_gather(normed, "tp", axis=0, tiled=True)
     outgoing = jnp.dot(pick, group, preferred_element_type=jnp.float32).astype(jnp.bfloat16)
     landed = lax.all_to_all(
         outgoing.reshape(ep_count, share, model_width), "ep", split_axis=0, concat_axis=0, tiled=True

time: 240 us -> 168 us (0.70)
  waiting for transfers between devices: 135 us -> 0.01 us
  Pallas kernels: 0 us -> 114 us
  blocking collectives: 38.2 us -> 6.62 us
  matrix products: 26.9 us -> 6.38 us
  between operations: 14 us -> 0.79 us
  local copies, waits for them, and re-layouts: 1.31 us -> 12.9 us
  other arithmetic: 15.1 us -> 21 us
  starting transfers between devices: 9.07 us -> 5.46 us
    pallas_call x0 -> x1, Pallas kernels: none -> 114 us  [run_exchange(): pl.pallas_call(functools.partial(exchange, ep_count=ep_count, share=share...]
    reduce_scatter x3 -> x0, waiting for transfers between devices: 56.7 us -> none  [the longest x1 27.8 us: local(): lax.psum_scatter(combined.astype(jnp.bfloat16), 'tp', scatter_dimension=0...]
    all_gather x2 -> x0, waiting for transfers between devices: 51.2 us -> none  [the longest x1 32.7 us: local(): incoming = lax.all_gather(landed, 'tp', axis=0, tiled=True)]
    all_to_all x1 -> x0, blocking collectives: 31.5 us -> none  [local(): lax.all_to_all(outgoing.reshape(ep_count, share, model_width), 'ep', spli...]
    all_to_all x1 -> x0, waiting for transfers between devices: 25.6 us -> none  [local(): lax.all_to_all(summed.reshape(ep_count, share, model_width), 'ep', split_...]
    dot_general x4 -> x0, matrix products: 19.8 us -> none  [the longest x1 10.1 us: local(): jnp.dot(hidden, down_proj[0], preferred_element_type=jnp.float32)]
    all_to_all x1 -> x0, starting transfers between devices: 5.5 us -> none  [local(): lax.all_to_all(summed.reshape(ep_count, share, model_width), 'ep', split_...]
    reduce_sum x1, other arithmetic: 11.2 us -> 14.3 us  [local(): jnp.sum(mixed, axis=1)]
  transfers between devices with their start and end apart: 7 -> 1, of which waited for: 7 -> 0; matrix products, arithmetic and copies ran while one was open for 9% -> 9% of each run, Pallas kernels for 0% -> 0%
where the time goes in v2:
time: 168 us; the launch traced here: 167 us
  Pallas kernels  114 us (68%)
  other arithmetic  21 us (12%)
  local copies, waits for them, and re-layouts  12.9 us (8%)
  blocking collectives  6.62 us (4%)
  matrix products  6.38 us (4%)
  starting transfers between devices  5.46 us (3%)
    pallas_call x1, Pallas kernels, run_exchange(): pl.pallas_call(functools.partial(exchange, ep_count=ep_count, share=share...  114 us
    reduce_sum x1, other arithmetic, local(): jnp.sum(mixed, axis=1)  14.3 us
    psum x1, blocking collectives, local(): lax.psum((jnp.sum(mixed, axis=1), jnp.sum(mixed * mixed, axis=1)), 'tp')  6.62 us
    dot_general x1, matrix products, local(): jnp.dot(activated, conv_proj, preferred_element_type=jnp.float32)  6.23 us
    ppermute x1, starting transfers between devices, shifted(): lax.ppermute(value, axis, [(source, source + steps) for source in range(l...  5.46 us
  transfers between devices with their start and end apart: 1, of which 0 were waited for; matrix products, arithmetic and copies ran while one was open for 9% of the time, Pallas kernels for 0%

profile of v2, /device:TPU:0, one launch (start us, length us, event | category | flops | bytes accessed | tf_op | source)
XLA Modules:
  0.0 167.1 jit_solution(9937486033095186585)
XLA Ops:
  0.6 0.0 copy-start
  0.6 0.0 copy-start.1
  0.7 1.5 slice.186
  2.2 5.5 %collective-permute-start = (bf16[30,512]{1,0:T(8,128)(2,1)}, bf16[30,512]{1,0:T(8,128)(2,1)}, u32[]{:S(2)}, u32[]{:S(2)}) collective-permute-start(bf16[30,512]{1,0:T(8,128)(2,1)} %slice.186), channel_id=1, source_target_pairs={{0,4},{4,8},{8,12},{12,16},{16,20},{20,24},{24,28},{1,5},{5,9},{9,... | collective-permute-start | bytes 92168 | tf_op jit(solution)/shard_map/ppermute | solution.py:329
  7.6 1.7 fusion.42
  9.3 0.7 and_select_fusion
  10.0 0.8 compare_reduce_fusion
  10.7 0.1 convolution_convert_fusion.1
  10.9 0.7 eq.39
  11.6 1.1 copy.21
  12.7 0.8 copy.22
  13.5 0.8 fusion.38
  14.3 0.7 broadcast_in_dim.24
  14.9 1.0 copy.23
  16.0 0.7 eq.42
  16.6 1.1 fusion.34
  17.7 1.8 %fusion.36.normed = bf16[64,2048]{1,0:T(8,128)(2,1)} fusion(bf16[64,2048]{1,0:T(8,128)(2,1)} %param.18, f32[2048]{0:T(1024)} %param.19, f32[64]{0:T(128)S(1)} %add_rsqrt_fusion.1), kind=kLoop, calls=%fused_computation.77 | loop fusion | flops 524288 | bytes 532736 | tf_op jit(solution)/shard_map/convert_element_type | solution.py:368
  19.5 1.6 fusion.37
  21.1 0.0 copy-start.3
  21.1 0.0 copy-start.4
  21.1 1.0 fusion.43
  22.1 0.7 copy.24.pick
  22.9 0.0 collective-permute-done
  22.9 0.0 copy-done.1
  22.9 14.3 %fusion.41 = (f32[1024]{0:T(1024)S(1)}, f32[1024]{0:T(1024)S(1)}, f32[1024,512]{1,0:T(8,128)}) fusion(f32[512]{0:T(512)S(1)} %bitcast.81, bf16[1024,512]{1,0:T(8,128)(2,1)S(1)} %copy-done.1, f32[512]{0:T(512)S(1)} %bitcast.80, bf16[30,512]{1,0:T(8,128)(2,1)} %collective-permute-done, f32[512]{0:T(512)S(1)} %bitcast.79, f32[512]{0:T(512)S(1)} %bitcast.78, ...), kind=kLoop, calls=%fused_computation.94 | loop fusion | flops 96991232 | bytes 3248128 | tf_op jit(solution)/shard_map/reduce_sum | solution.py:357
  37.2 6.6 %all-reduce = (f32[1024]{0:T(1024)S(1)}, f32[1024]{0:T(1024)S(1)}) all-reduce(f32[1024]{0:T(1024)S(1)} %get-tuple-element.3, f32[1024]{0:T(1024)S(1)} %get-tuple-element.2), channel_id=1, replica_groups=mesh['ep'=8,'tp'=4] {'tp'}, use_global_device_ids=true, to_apply=%region_6.7 | all-reduce | flops 2048 | bytes 16384 | tf_op jit(solution)/shard_map/psum | solution.py:357
  43.8 0.0 copy-done
  43.9 0.0 copy-done.3
  43.9 0.0 copy-done.4
  43.9 6.2 %convolution_convert_fusion.partial = bf16[1024,2048]{1,0:T(8,128)(2,1)} fusion(bf16[512,2048]{1,0:T(8,128)(2,1)S(1)} %copy-done, f32[1024,512]{1,0:T(8,128)} %get-tuple-element.6, f32[512]{0:T(512)S(1)} %copy-done.3, f32[512]{0:T(512)S(1)} %copy-done.4, f32[1024]{0:T(1024)S(1)} %get-tuple-element.41, f32[1024]{0:T(1024)S(1)} %get-tuple-element.40), kind=kOutput, calls=%fused_computation.29 | convolution fusion | flops 2154299392 | bytes 8400896 | tf_op jit(solution)/shard_map/dot_general | solution.py:362
  50.1 114.0 %shard_map.140 = (bf16[256,2048]{1,0:T(8,128)(2,1)}, bf16[64,2048]{1,0:T(8,128)(2,1)}) custom-call(bf16[64,2048]{1,0:T(8,128)(2,1)} %fusion.36.normed, bf16[256,256]{1,0:T(8,128)(2,1)} %copy.24.pick, bf16[256,256]{1,0:T(8,128)(2,1)} %get-tuple-element.7.scale, bf16[1024,2048]{1,0:T(8,128)(2,1)} %convolution_convert_fusion.partial, ...), custom_call_target="tpu_custom_call" | custom-call | tf_op jit(solution)/shard_map/pallas_call | solution.py:282
  164.1 0.0 copy-start.2
  164.1 2.3 %copy.27 = bf16[256,2048]{1,0:T(8,128)(2,1)} copy(bf16[256,2048]{1,0:T(8,128)(2,1)} %get-tuple-element.44) | data formatting | bytes 2097152
  166.4 0.0 copy-done.2
  166.4 0.7 copy.28
  (6 shorter events, 0.1 us)
Async XLA Ops:
  0.6 43.2 %copy-start = (bf16[512,2048]{1,0:T(8,128)(2,1)S(1)}, bf16[512,2048]{1,0:T(8,128)(2,1)}, u32[]{:S(2)}) copy-start(bf16[512,2048]{1,0:T(8,128)(2,1)} %param.17) | copy-start | bytes 6291460
  0.6 22.2 %copy-start.1 = (bf16[1024,512]{1,0:T(8,128)(2,1)S(1)}, bf16[1024,512]{1,0:T(8,128)(2,1)}, u32[]{:S(2)}) copy-start(bf16[1024,512]{1,0:T(8,128)(2,1)} %param.13) | copy-start | bytes 3145732
  2.2 20.7 %collective-permute-start = (bf16[30,512]{1,0:T(8,128)(2,1)}, bf16[30,512]{1,0:T(8,128)(2,1)}, u32[]{:S(2)}, u32[]{:S(2)}) collective-permute-start(bf16[30,512]{1,0:T(8,128)(2,1)} %slice.186), channel_id=1, source_target_pairs={{0,4},{4,8},{8,12},{12,16},{16,20},{20,24},{24,28},{1,5},{5,9},{9,... | collective-permute-start | bytes 92168 | tf_op jit(solution)/shard_map/ppermute | solution.py:329
  21.1 22.7 %copy-start.3 = (f32[512]{0:T(512)S(1)}, f32[512]{0:T(512)}, u32[]{:S(2)}) copy-start(f32[512]{0:T(512)} %param.16) | copy-start | bytes 6148
  21.1 22.8 %copy-start.4 = (f32[512]{0:T(512)S(1)}, f32[512]{0:T(512)}, u32[]{:S(2)}) copy-start(f32[512]{0:T(512)} %param.15) | copy-start | bytes 6148
  164.1 2.4 %copy-start.2 = (bf16[64,2048]{1,0:T(8,128)(2,1)S(1)}, bf16[64,2048]{1,0:T(8,128)(2,1)}, u32[]{:S(2)}) copy-start(bf16[64,2048]{1,0:T(8,128)(2,1)} %get-tuple-element.45) | copy-start | bytes 786436

commit v3 on v2

--- a/solution.py
+++ b/solution.py
@@ -19,11 +19,11 @@
 
 
 def exchange(
-    normed, pick, scale, partial, gate_hbm, up_hbm, down_hbm,
+    normed, ranks, weights, mixed, stats, gain, shift, proj, gate_hbm, up_hbm, down_hbm,
     conv_out, moe_out,
-    gate, up, down, group, outgoing, arrived, pieces, from_core, to_y, from_y, to_ep, returned,
+    partial, stats_in, columns, gate, up, down, group, outgoing, arrived, pieces, from_core, to_y, from_y, to_ep, returned,
     conv_core, conv_to_y, conv_from_y, combined, last_core, last_to_y, last_from_y,
-    weight_sem, ag_send, ag_recv, ep_send, ep_recv, fan_send, fan_recv,
+    weight_sem, stats_send, stats_recv, ag_send, ag_recv, ep_send, ep_recv, fan_send, fan_recv,
     core_send, core_recv, y_send, y_recv, back_send, back_recv,
     conv_send, conv_recv, last_send, last_recv,
     *, ep_count, share,
@@ -54,11 +54,12 @@
     barrier = pltpu.get_barrier_semaphore()
     pl.semaphore_signal(barrier, inc=1, device_id={"tp": core}, device_id_type=MESH)
     pl.semaphore_signal(barrier, inc=1, device_id={"tp": over}, device_id_type=MESH)
+    pl.semaphore_signal(barrier, inc=1, device_id={"tp": far}, device_id_type=MESH)
     for d in range(1, ep_count):
         pl.semaphore_signal(
             barrier, inc=1, device_id={"ep": (me_ep + d) % ep_count}, device_id_type=MESH
         )
-    pl.semaphore_wait(barrier, ep_count + 1)
+    pl.semaphore_wait(barrier, ep_count + 2)
 
     sent = []
 
@@ -67,8 +68,15 @@
         remote(normed, block(group, me, rows), ag_send.at[1], ag_recv.at[1], {"tp": core}),
         remote(block(group, over, rows), block(group, over, rows), ag_send.at[2], ag_recv.at[2], {"tp": core}),
     ]
+    moments = [
+        remote(stats, stats_in.at[n], stats_send.at[n], stats_recv.at[n], {"tp": where})
+        for n, where in enumerate((over, core, far))
+    ]
+    sent += moments
     ag[0].start()
     ag[1].start()
+    for r in moments:
+        r.start()
     group[pl.ds(pl.multiple_of(me * rows, rows), rows), :] = normed[...]
     span = partial.shape[0] // 4
     conv = [
@@ -80,15 +88,17 @@
     ]
     ag[0].wait_recv()
     ag[2].start()
-    conv[1].start()
-    conv[0].start()
     ag[1].wait_recv()
     ag[2].wait_recv()
     sent += ag + conv
 
     tile = 512
+    group_rows = ranks.shape[1]
+    wanted = me * share + lax.broadcasted_iota(jnp.int32, (share, group_rows), 0)
+    held = [ranks[s : s + 1, :] == wanted for s in range(ep_count)]
+    pick = jnp.concatenate([jnp.where(h, 1.0, 0.0) for h in held], axis=0).astype(bf16)
     for n in range(0, width, tile):
-        part = jnp.dot(pick[...], group[:, n : n + tile], preferred_element_type=f32).astype(bf16)
+        part = jnp.dot(pick, group[:, n : n + tile], preferred_element_type=f32).astype(bf16)
         outgoing[:, n : n + tile] = part
         arrived[pl.ds(pl.multiple_of(me * share, share), share), n : n + tile] = part[:share]
     ep = []
@@ -101,6 +111,26 @@
         )
         ep[-1].start()
     sent += ep
+
+    def center_and_scale():
+        for r in moments:
+            r.wait_recv()
+        total = (stats[...] + stats_in[0] + stats_in[1] + stats_in[2]) / width
+        center = total[0:1, :]
+        spread = jnp.maximum(total[1:2, :] - center * center, 0.0)
+        both = jnp.concatenate([center, lax.rsqrt(spread + 1e-05)] + [center] * 6, axis=0)
+        columns[...] = both.T
+
+    def project(quarter):
+        at = pl.multiple_of(quarter * span, span)
+        view = pl.ds(at, span)
+        col = columns[view, :]
+        scaled = (mixed[view, :] - col[:, 0:1]) * col[:, 1:2] * gain[...] + shift[...]
+        activated = (scaled / (1.0 + jnp.exp(-scaled))).astype(bf16)
+        for n in range(0, width, tile):
+            partial[view, n : n + tile] = jnp.dot(
+                activated, proj[:, n : n + tile], preferred_element_type=f32
+            ).astype(bf16)
 
     def fan(kind, s):
         quarter = over if kind == 2 else me
@@ -212,6 +242,17 @@
         land(s)
         if s >= 2:
             relay(s - 2)
+        if s == 1:
+            center_and_scale()
+            project(far)
+            conv[1].start()
+        if s == 2:
+            project(core)
+            conv[0].start()
+        if s == 3:
+            project(over)
+        if s == 4:
+            project(me)
         if s == 3:
             for load in loads:
                 load.wait()
@@ -241,9 +282,12 @@
 
     for r in backs:
         r.wait_recv()
+    scale = jnp.concatenate(
+        [jnp.where(h, weights[s : s + 1, :], 0.0) for s, h in enumerate(held)], axis=0
+    ).T.astype(bf16)
     for n in range(0, width, tile):
         combined[:, n : n + tile] = jnp.dot(
-            scale[...], returned[:, n : n + tile], preferred_element_type=f32
+            scale, returned[:, n : n + tile], preferred_element_type=f32
         ).astype(bf16)
     last = [
         remote(
@@ -271,10 +315,13 @@
         r.wait_send()
 
 
-def run_exchange(normed, pick, scale, partial, gate, up, down, ep_count, share):
+def run_exchange(
+    normed, ranks, weights, mixed, stats, gain, shift, proj, gate, up, down, ep_count, share
+):
     rows, width = normed.shape
     hid = gate.shape[1]
-    span = partial.shape[0] // 4
+    conv_rows = mixed.shape[0]
+    span = conv_rows // 4
     bf16 = jnp.bfloat16
     slots = ep_count * share
     vmem, dma = pltpu.VMEM, pltpu.SemaphoreType.DMA
@@ -285,9 +332,12 @@
             jax.ShapeDtypeStruct((span, width), bf16),
             jax.ShapeDtypeStruct((rows, width), bf16),
         ),
-        in_specs=[at_vmem] * 4 + [at_any] * 3,
+        in_specs=[at_vmem] * 8 + [at_any] * 3,
         out_specs=(at_vmem, at_vmem),
         scratch_shapes=[
+            vmem((conv_rows, width), bf16),
+            vmem((3, 8, conv_rows), jnp.float32),
+            vmem((conv_rows, 8), jnp.float32),
             vmem((width, hid), bf16),
             vmem((width, hid), bf16),
             vmem((hid, width), bf16),
@@ -309,6 +359,7 @@
             vmem((rows, width), bf16),
             dma((3,)),
             dma((3,)), dma((3,)),
+            dma((3,)), dma((3,)),
             dma((ep_count,)), dma((ep_count,)),
             dma((3, ep_count)), dma((3, ep_count)),
             dma((ep_count, 2)), dma((ep_count, 2)),
@@ -320,7 +371,7 @@
         compiler_params=pltpu.CompilerParams(
             collective_id=0, has_side_effects=True, vmem_limit_bytes=60 * 1024 * 1024
         ),
-    )(normed, pick, scale, partial, gate, up, down)
+    )(normed, ranks, weights, mixed, stats, gain, shift, proj, gate, up, down)
 
 
 def shifted(value, axis, steps):
@@ -353,13 +404,7 @@
     mixed = jnp.zeros((local_rows, local_width), jnp.float32)
     for offset in range(reach + 1):
         mixed = mixed + padded[offset : offset + local_rows].astype(jnp.float32) * taps[offset]
-    full_width = local_width * tp_count
-    sums, squares = lax.psum((jnp.sum(mixed, axis=1), jnp.sum(mixed * mixed, axis=1)), "tp")
-    center = sums / full_width
-    spread = jnp.maximum(squares / full_width - center * center, 0.0)
-    scaled = (mixed - center[:, None]) * lax.rsqrt(spread[:, None] + 1e-05) * norm_gain + norm_shift
-    activated = jax.nn.silu(scaled).astype(jnp.bfloat16)
-    partial = jnp.dot(activated, conv_proj, preferred_element_type=jnp.float32).astype(jnp.bfloat16)
+    row_sums, row_squares = jnp.sum(mixed, axis=1), jnp.sum(mixed * mixed, axis=1)
     moe_float = moe_input.astype(jnp.float32)
     normed = (
         moe_float
@@ -384,6 +429,21 @@
     rank = jnp.dot(hit.astype(jnp.bfloat16), before, preferred_element_type=jnp.float32).astype(
         jnp.int32
     )
+    if direct:
+        ranks = jnp.where(hit, rank, -1)
+        idle = jnp.zeros((6, local_rows), jnp.float32)
+        stats = jnp.concatenate([row_sums[None, :], row_squares[None, :], idle], axis=0)
+        return run_exchange(
+            normed, ranks, weight, mixed, stats, norm_gain[None, :], norm_shift[None, :],
+            conv_proj, gate_proj[0], up_proj[0], down_proj[0], ep_count, share,
+        )
+    full_width = local_width * tp_count
+    sums, squares = lax.psum((row_sums, row_squares), "tp")
+    center = sums / full_width
+    spread = jnp.maximum(squares / full_width - center * center, 0.0)
+    scaled = (mixed - center[:, None]) * lax.rsqrt(spread[:, None] + 1e-05) * norm_gain + norm_shift
+    activated = jax.nn.silu(scaled).astype(jnp.bfloat16)
+    partial = jnp.dot(activated, conv_proj, preferred_element_type=jnp.float32).astype(jnp.bfloat16)
     first = lax.axis_index("tp") * share
     slots = first + jnp.arange(share, dtype=jnp.int32)
     held = hit[:, None, :] & (rank[:, None, :] == slots[None, :, None])
@@ -393,10 +453,6 @@
         .astype(jnp.bfloat16)
         .reshape(ep_count * share, group_rows)
     )
-    if direct:
-        return run_exchange(
-            normed, pick, scale.T, partial, gate_proj[0], up_proj[0], down_proj[0], ep_count, share
-        )
     conv_out = lax.psum_scatter(partial, "tp", scatter_dimension=0, tiled=True)
     group = lax.all_gather(normed, "tp", axis=0, tiled=True)
     outgoing = jnp.dot(pick, group, preferred_element_type=jnp.float32).astype(jnp.bfloat16)

time: 168 us -> 161 us (0.958)
  other arithmetic: 21 us -> 32.8 us
  local copies, waits for them, and re-layouts: 12.9 us -> 5.92 us
  blocking collectives: 6.62 us -> 0 us
  matrix products: 6.38 us -> 0.75 us
  Pallas kernels: 114 us -> 116 us
    reduce_sum x1, other arithmetic: 14.3 us -> 26.5 us  [local(): jnp.sum(mixed, axis=1)]
    psum x1 -> x0, blocking collectives: 6.62 us -> none  [local(): lax.psum((jnp.sum(mixed, axis=1), jnp.sum(mixed * mixed, axis=1)), 'tp')]
    dot_general x1 -> x0, matrix products: 6.23 us -> none  [local(): jnp.dot(activated, conv_proj, preferred_element_type=jnp.float32)]
    eq x4 -> x0, local copies, waits for them, and re-layouts: 2.46 us -> none  [local(): held = hit[:, None, :] & (rank[:, None, :] == slots[None, :, None])]
    pallas_call x1, Pallas kernels: 114 us -> 116 us  [run_exchange(): pl.pallas_call(functools.partial(exchange, ep_count=ep_count, share=share...]
  transfers between devices with their start and end apart: 1 -> 1, of which waited for: 0 -> 0; matrix products, arithmetic and copies ran while one was open for 9% -> 5% of each run, Pallas kernels for 0% -> 0%
where the time goes in v3:
time: 161 us
  Pallas kernels  116 us (72%)
  other arithmetic  32.8 us (20%)
  local copies, waits for them, and re-layouts  5.92 us (4%)
  starting transfers between devices  4.87 us (3%)
    pallas_call x1, Pallas kernels, run_exchange(): pl.pallas_call(functools.partial(exchange, ep_count=ep_count, share=share...  116 us
    reduce_sum x1, other arithmetic, local(): jnp.sum(mixed, axis=1)  26.5 us
    ppermute x1, starting transfers between devices, shifted(): lax.ppermute(value, axis, [(source, source + steps) for source in range(l...  4.87 us
  transfers between devices with their start and end apart: 1, of which 0 were waited for; matrix products, arithmetic and copies ran while one was open for 5% of the time, Pallas kernels for 0%

profile of v3, /device:TPU:0, one launch (start us, length us, event | category | flops | bytes accessed | tf_op | source)
XLA Modules:
  0.0 160.8 jit_solution(17487434484874776914)
XLA Ops:
  0.6 0.8 slice.186
  1.4 4.9 %collective-permute-start = (bf16[30,512]{1,0:T(8,128)(2,1)S(1)}, bf16[30,512]{1,0:T(8,128)(2,1)S(1)}, u32[]{:S(2)}, u32[]{:S(2)}) collective-permute-start(bf16[30,512]{1,0:T(8,128)(2,1)S(1)} %slice.186), channel_id=1, source_target_pairs={{0,4},{4,8},{8,12},{12,16},{16,20},{20,24},{24,28},{1,5},{5,9},{9,... | collective-permute-start | bytes 92168 | tf_op jit(solution)/shard_map/ppermute | solution.py:380
  6.3 1.0 fusion.37
  7.3 1.0 fusion.36
  8.3 1.1 fusion.30
  9.4 0.7 and_select_fusion
  10.1 0.8 compare_reduce_fusion
  10.9 0.8 fusion.ranks
  11.6 1.8 %fusion.32.normed = bf16[64,2048]{1,0:T(8,128)(2,1)} fusion(bf16[64,2048]{1,0:T(8,128)(2,1)} %param.18, f32[2048]{0:T(1024)} %param.19, f32[64]{0:T(128)S(1)} %add_rsqrt_fusion), kind=kLoop, calls=%fused_computation.71 | loop fusion | flops 524288 | bytes 532736 | tf_op jit(solution)/shard_map/convert_element_type | solution.py:413
  13.4 1.4 fusion.33.weights
  14.8 0.1 pad.2.clone
  14.8 0.0 collective-permute-done
  14.8 26.5 %fusion.35 = (f32[1024]{0:T(1024)S(1)}, f32[1024]{0:T(1024)S(1)}, f32[1024,512]{1,0:T(8,128)}) fusion(f32[512]{0:T(512)S(1)} %bitcast.59, bf16[1024,512]{1,0:T(8,128)(2,1)} %param.13, f32[512]{0:T(512)S(1)} %bitcast.58, bf16[30,512]{1,0:T(8,128)(2,1)S(1)} %collective-permute-done, f32[512]{0:T(512)S(1)} %bitcast.57, f32[512]{0:T(512)S(1)} %bitcast.56, ...), kind=kLoop, calls=%fused_computation.82 | loop fusion | flops 96991232 | bytes 3248128 | tf_op jit(solution)/shard_map/reduce_sum | solution.py:407
  41.3 0.7 maximum_maximum_fusion.stats
  42.0 115.7 %shard_map.140 = (bf16[256,2048]{1,0:T(8,128)(2,1)}, bf16[64,2048]{1,0:T(8,128)(2,1)}) custom-call(bf16[64,2048]{1,0:T(8,128)(2,1)} %fusion.32.normed, s32[8,256]{1,0:T(8,128)} %fusion.ranks, f32[8,256]{1,0:T(8,128)} %fusion.33.weights, f32[1024,512]{1,0:T(8,128)} %get-tuple-element.4.mixed, f32[8,1024]{1,0:T(8,128)} %maximum_maximum_fusion.stats, ...), custom_call_target="tpu_custom_call" | custom-call | tf_op jit(solution)/shard_map/pallas_call | solution.py:329
  157.7 0.0 copy-start
  157.7 2.3 %copy.17 = bf16[256,2048]{1,0:T(8,128)(2,1)} copy(bf16[256,2048]{1,0:T(8,128)(2,1)} %get-tuple-element.38) | data formatting | bytes 2097152
  160.1 0.0 copy-done
  160.1 0.7 copy.18
  (2 shorter events, 0.0 us)
Async XLA Ops:
  1.4 13.4 %collective-permute-start = (bf16[30,512]{1,0:T(8,128)(2,1)S(1)}, bf16[30,512]{1,0:T(8,128)(2,1)S(1)}, u32[]{:S(2)}, u32[]{:S(2)}) collective-permute-start(bf16[30,512]{1,0:T(8,128)(2,1)S(1)} %slice.186), channel_id=1, source_target_pairs={{0,4},{4,8},{8,12},{12,16},{16,20},{20,24},{24,28},{1,5},{5,9},{9,... | collective-permute-start | bytes 92168 | tf_op jit(solution)/shard_map/ppermute | solution.py:380
  157.7 2.4 %copy-start = (bf16[64,2048]{1,0:T(8,128)(2,1)S(1)}, bf16[64,2048]{1,0:T(8,128)(2,1)}, u32[]{:S(2)}) copy-start(bf16[64,2048]{1,0:T(8,128)(2,1)} %get-tuple-element.39) | copy-start | bytes 786436
